TPU v7x, 1024 devices: a whole 4x8x16 slice. The times are simulated.
1024 devices in a mesh: ra: 16 (over z), cb: 8 (over y), dp: 8 (over x, core).
Axes of the slice: x: 4, y: 8, z: 16, core: 2. Of those that a mesh axis runs over, the one named last changes fastest.
Arguments:
- stream: bfloat16 [2048, 2048], P('dp', 'ra'), may hold values from -60 to 60
- norm_gain: float32 [2, 2048], P(None, 'ra'), may hold values from 0.1 to 1.9
- gate_weight: float32 [2, 2048, 5504], P(None, 'ra', 'cb'), may hold values from -0.125 to 0.125
- up_weight: float32 [2, 2048, 5504], P(None, 'ra', 'cb'), may hold values from -0.125 to 0.125
- down_weight: float32 [2, 5504, 2048], P(None, 'cb', 'ra'), may hold values from -0.078125 to 0.078125
- gate_scale: float32 [2, 5504], P(None, 'cb'), may hold values from 0.5 to 2
- up_scale: float32 [2, 5504], P(None, 'cb'), may hold values from 0.5 to 2
- down_scale: float32 [2, 2048], P(None, 'ra'), may hold values from 0.5 to 2
Outputs:
- result: bfloat16 [2048, 2048], P('dp', 'ra')
All inputs are finite; a program needn't handle non-finite values.
Results may differ from a plain program's by a relative error of at most 0.04.
Values may be sent and summed in bfloat16 or wider, within the bound.
A program may use at most 32 MiB of HBM per device.

v0:
```python
import jax
import jax.numpy as jnp
from jax import lax
from jax.sharding import PartitionSpec as P

D = 2048


epsilon = 1e-06
residual_scale = 0.5


def sent_to_all(x, axis):
    copies = jnp.broadcast_to(x, (lax.axis_size(axis), *x.shape))
    return lax.all_to_all(copies, axis, split_axis=0, concat_axis=0, tiled=True)


def of_everyone(x, axis):
    return sent_to_all(x, axis).sum(axis=0)


def cut_along(x, dim, peers):
    shape = x.shape
    tiles = x.reshape(*shape[:dim], peers, shape[dim] // peers, *shape[dim + 1 :])
    return jnp.moveaxis(tiles, dim, 0)


def sum_at_owner(x, axis, dim):
    tiles = cut_along(x, dim, lax.axis_size(axis))
    arrived = lax.all_to_all(tiles, axis, split_axis=0, concat_axis=0, tiled=True)
    return arrived.astype(jnp.float32).sum(axis=0)


def in_one_piece(arrays, axis, dim, along):
    widths = [a.shape[along] for a in arrays]
    both = jnp.concatenate(arrays, axis=along)
    whole = sum_at_owner(both, axis, dim)
    return tuple(jnp.split(whole, [sum(widths[:k]) for k in range(1, len(widths))], axis=along))


def activate(gate_part, up_part, squares, gate_scale, up_scale):
    inverse = lax.rsqrt(squares / D + epsilon)
    gate_sum = gate_part * inverse * gate_scale
    up_sum = up_part * inverse * up_scale
    return (jax.nn.silu(gate_sum) * up_sum).astype(jnp.bfloat16)


def half_step(stream, gain, gate_weight, up_weight, down_weight, gate_scale, up_scale, down_scale):
    widened = stream.astype(jnp.float32)
    local_squares = jnp.sum(widened * widened, axis=1, keepdims=True)
    normed = (widened * gain).astype(jnp.bfloat16)
    gate_part = jnp.dot(
        normed, gate_weight.astype(jnp.bfloat16), preferred_element_type=jnp.float32
    ).astype(jnp.bfloat16)
    up_part = jnp.dot(
        normed, up_weight.astype(jnp.bfloat16), preferred_element_type=jnp.float32
    ).astype(jnp.bfloat16)
    total_squares = of_everyone(local_squares, "ra")
    summed = in_one_piece((gate_part, up_part), "ra", 0, 1)
    share_rows = summed[0].shape[0]
    squares = lax.dynamic_slice_in_dim(
        total_squares, lax.axis_index("ra") * share_rows, share_rows, 0
    )
    own_hidden = activate(summed[0], summed[1], squares, gate_scale, up_scale)
    hidden = lax.all_gather(own_hidden, "ra", axis=0, tiled=True)
    partial_down = jnp.dot(
        hidden, down_weight.astype(jnp.bfloat16), preferred_element_type=jnp.float32
    )
    branch = of_everyone(partial_down, "cb") * down_scale
    return (residual_scale * widened + branch).astype(jnp.bfloat16)


def on_device(
    stream, norm_gain, gate_weight, up_weight, down_weight, gate_scale, up_scale, down_scale
):
    current = stream
    for block_index in range(2):
        current = half_step(
            current,
            norm_gain[block_index],
            gate_weight[block_index],
            up_weight[block_index],
            down_weight[block_index],
            gate_scale[block_index],
            up_scale[block_index],
            down_scale[block_index],
        )
    return current


def solution(mesh):
    in_specs = (
        P("dp", "ra"),
        P(None, "ra"),
        P(None, "ra", "cb"),
        P(None, "ra", "cb"),
        P(None, "cb", "ra"),
        P(None, "cb"),
        P(None, "cb"),
        P(None, "ra"),
    )
    out_specs = P("dp", "ra")
    return jax.shard_map(
        on_device, mesh=mesh, in_specs=in_specs, out_specs=out_specs, check_vma=False
    )
```

profile of v0, /device:TPU:4, one launch (start us, length us, event | category | flops | bytes accessed | tf_op | source)
XLA Modules:
  0.0 240.8 jit_solution(18148925239128583850)
XLA Ops:
  0.0 0.0 copy-start.1
  0.0 1.0 fusion.5
  1.0 0.6 broadcast_in_dim.14
  1.6 18.9 %all-to-all-start.1 = ((f32[16,256,1]{1,2,0:T(1,128)}), f32[16,256,1]{1,2,0:T(1,128)S(1)}, u32[]{:S(2)}, u32[]{:S(2)}) async-start(f32[16,256,1]{1,2,0:T(1,128)} %broadcast_in_dim.14), calls=%async_computation.1 | async-start | bytes 32768 | tf_op jit(solution)/shard_map/all_to_all | solution.py:15
  20.5 0.8 slice_bitcast_fusion.13
  21.3 0.0 copy-start
  21.3 1.2 convert.13
  22.5 0.0 copy-done.1
  22.5 0.0 copy-done
  22.5 0.3 convolution_convert_fusion.2
  22.8 0.3 convolution_convert_fusion.3
  23.1 1.1 copy.13
  24.2 0.0 copy-start.2
  24.3 8.8 %all-to-all-done.1 = f32[16,256,1]{1,2,0:T(1,128)S(1)} async-done(((f32[16,256,1]{1,2,0:T(1,128)}), f32[16,256,1]{1,2,0:T(1,128)S(1)}, u32[]{:S(2)}, u32[]{:S(2)}) %all-to-all-start.1) | async-done | bytes 16416 | tf_op jit(solution)/shard_map/all_to_all | solution.py:15
  33.0 0.0 copy-start.3
  33.0 0.0 copy-start.4
  33.0 3.7 %all-to-all-start = ((bf16[16,16,1376]{2,1,0:T(8,128)(2,1)}), bf16[16,16,1376]{2,1,0:T(8,128)(2,1)S(1)}, u32[]{:S(2)}, u32[]{:S(2)}) async-start(bf16[16,16,1376]{2,1,0:T(8,128)(2,1)} %bitcast.3), calls=%async_computation | async-start | bytes 1441792 | tf_op jit(solution)/shard_map/all_to_all | solution.py:30
  36.8 0.0 copy-done.2
  36.8 0.0 copy-done.3
  36.9 0.0 copy-done.4
  36.9 0.1 add_rsqrt_fusion.1
  37.0 35.0 %all-to-all-done = bf16[16,16,1376]{2,1,0:T(8,128)(2,1)S(1)} async-done(((bf16[16,16,1376]{2,1,0:T(8,128)(2,1)}), bf16[16,16,1376]{2,1,0:T(8,128)(2,1)S(1)}, u32[]{:S(2)}, u32[]{:S(2)}) %all-to-all-start) | async-done | bytes 704544 | tf_op jit(solution)/shard_map/all_to_all | solution.py:30
  72.0 0.1 convert_reduce_fusion.1
  72.1 0.1 fusion.20
  72.2 33.7 %all_gather.6 = bf16[256,688]{1,0:T(8,128)(2,1)S(1)} all-gather(bf16[16,688]{1,0:T(8,128)(2,1)S(1)} %fusion.20), channel_id=1, replica_groups=mesh['ra'=16,'cb'=8,'dp'=8] {'ra'}, dimensions={0}, use_global_device_ids=true | all-gather | bytes 374272 | tf_op jit(solution)/shard_map/all_gather | solution.py:65
  105.9 0.3 fusion.1
  106.1 1.1 broadcast_in_dim.15
  107.2 0.0 copy-start.5
  107.2 7.2 %all-to-all-start.2 = ((f32[8,256,128]{2,1,0:T(8,128)}), f32[8,256,128]{2,1,0:T(8,128)S(1)}, u32[]{:S(2)}, u32[]{:S(2)}) async-start(f32[8,256,128]{2,1,0:T(8,128)} %broadcast_in_dim.15), calls=%async_computation.2 | async-start | bytes 2097152 | tf_op jit(solution)/shard_map/all_to_all | solution.py:15
  114.4 0.0 copy-done.5
  114.4 17.7 %all-to-all-done.2 = f32[8,256,128]{2,1,0:T(8,128)S(1)} async-done(((f32[8,256,128]{2,1,0:T(8,128)}), f32[8,256,128]{2,1,0:T(8,128)S(1)}, u32[]{:S(2)}, u32[]{:S(2)}) %all-to-all-start.2) | async-done | bytes 1048608 | tf_op jit(solution)/shard_map/all_to_all | solution.py:15
  132.1 0.1 reduce_sum.75
  132.2 0.1 fusion.9
  132.3 0.3 convolution_convert_fusion.1
  132.6 0.3 convolution_convert_fusion
  132.8 0.6 broadcast_in_dim.16
  133.5 8.5 %all-to-all-start.4 = ((f32[16,256,1]{1,2,0:T(1,128)}), f32[16,256,1]{1,2,0:T(1,128)S(1)}, u32[]{:S(2)}, u32[]{:S(2)}) async-start(f32[16,256,1]{1,2,0:T(1,128)} %broadcast_in_dim.16), calls=%async_computation.4 | async-start | bytes 32768 | tf_op jit(solution)/shard_map/all_to_all | solution.py:15
  142.0 1.1 copy.14
  143.2 11.4 %all-to-all-done.4 = f32[16,256,1]{1,2,0:T(1,128)S(1)} async-done(((f32[16,256,1]{1,2,0:T(1,128)}), f32[16,256,1]{1,2,0:T(1,128)S(1)}, u32[]{:S(2)}, u32[]{:S(2)}) %all-to-all-start.4) | async-done | bytes 16416 | tf_op jit(solution)/shard_map/all_to_all | solution.py:15
  154.5 3.6 %all-to-all-start.3 = ((bf16[16,16,1376]{2,1,0:T(8,128)(2,1)}), bf16[16,16,1376]{2,1,0:T(8,128)(2,1)S(1)}, u32[]{:S(2)}, u32[]{:S(2)}) async-start(bf16[16,16,1376]{2,1,0:T(8,128)(2,1)} %bitcast.9), calls=%async_computation.3 | async-start | bytes 1441792 | tf_op jit(solution)/shard_map/all_to_all | solution.py:30
  158.2 0.1 add_rsqrt_fusion
  158.2 27.1 %all-to-all-done.3 = bf16[16,16,1376]{2,1,0:T(8,128)(2,1)S(1)} async-done(((bf16[16,16,1376]{2,1,0:T(8,128)(2,1)}), bf16[16,16,1376]{2,1,0:T(8,128)(2,1)S(1)}, u32[]{:S(2)}, u32[]{:S(2)}) %all-to-all-start.3) | async-done | bytes 704544 | tf_op jit(solution)/shard_map/all_to_all | solution.py:30
  185.3 0.1 convert_reduce_fusion
  185.4 0.1 fusion.16
  185.5 32.9 %all_gather.7 = bf16[256,688]{1,0:T(8,128)(2,1)S(1)} all-gather(bf16[16,688]{1,0:T(8,128)(2,1)S(1)} %fusion.16), channel_id=1, replica_groups=mesh['ra'=16,'cb'=8,'dp'=8] {'ra'}, dimensions={0}, use_global_device_ids=true | all-gather | bytes 374272 | tf_op jit(solution)/shard_map/all_gather | solution.py:65
  218.4 0.2 fusion
  218.7 0.1 broadcast_in_dim.17
  218.7 21.3 %all_to_all.30 = f32[8,256,128]{2,1,0:T(8,128)S(1)} all-to-all(f32[8,256,128]{2,1,0:T(8,128)S(1)} %broadcast_in_dim.17), channel_id=1, replica_groups=mesh['ra'=16,'cb'=8,'dp'=8] {'cb'}, dimensions={0} | all-to-all | bytes 2097152 | tf_op jit(solution)/shard_map/all_to_all | solution.py:15
  240.1 0.1 reduce_sum.79
  240.1 0.7 fusion.7
  (8 shorter events, 0.3 us)
Async XLA Ops:
  0.0 22.5 %copy-start.1 = (f32[2,128,688]{1,2,0:T(8,128)S(1)}, f32[2,128,688]{1,2,0:T(8,128)}, u32[]{:S(2)}) copy-start(f32[2,128,688]{1,2,0:T(8,128)} %param.10) | copy-start | bytes 2113540
  1.6 31.4 %all-to-all-start.1 = ((f32[16,256,1]{1,2,0:T(1,128)}), f32[16,256,1]{1,2,0:T(1,128)S(1)}, u32[]{:S(2)}, u32[]{:S(2)}) async-start(f32[16,256,1]{1,2,0:T(1,128)} %broadcast_in_dim.14), calls=%async_computation.1 | async-start | bytes 32768 | tf_op jit(solution)/shard_map/all_to_all | solution.py:15
  21.3 1.3 copy-start
  24.2 12.5 %copy-start.2 = (f32[2,688,128]{2,1,0:T(8,128)S(1)}, f32[2,688,128]{2,1,0:T(8,128)}, u32[]{:S(2)}) copy-start(f32[2,688,128]{2,1,0:T(8,128)} %param.12) | copy-start | bytes 2113540
  33.0 3.8 %copy-start.3 = (f32[2,688]{1,0:T(2,128)S(1)}, f32[2,688]{1,0:T(2,128)}, u32[]{:S(2)}) copy-start(f32[2,688]{1,0:T(2,128)} %param.14) | copy-start | bytes 16516
  33.0 3.8 %copy-start.4 = (f32[2,688]{1,0:T(2,128)S(1)}, f32[2,688]{1,0:T(2,128)}, u32[]{:S(2)}) copy-start(f32[2,688]{1,0:T(2,128)} %param.13) | copy-start | bytes 16516
  33.0 39.0 %all-to-all-start = ((bf16[16,16,1376]{2,1,0:T(8,128)(2,1)}), bf16[16,16,1376]{2,1,0:T(8,128)(2,1)S(1)}, u32[]{:S(2)}, u32[]{:S(2)}) async-start(bf16[16,16,1376]{2,1,0:T(8,128)(2,1)} %bitcast.3), calls=%async_computation | async-start | bytes 1441792 | tf_op jit(solution)/shard_map/all_to_all | solution.py:30
  107.2 7.2 %copy-start.5 = (f32[2,128]{1,0:T(2,128)S(1)}, f32[2,128]{1,0:T(2,128)}, u32[]{:S(2)}) copy-start(f32[2,128]{1,0:T(2,128)} %param.15) | copy-start | bytes 3076
  107.2 24.9 %all-to-all-start.2 = ((f32[8,256,128]{2,1,0:T(8,128)}), f32[8,256,128]{2,1,0:T(8,128)S(1)}, u32[]{:S(2)}, u32[]{:S(2)}) async-start(f32[8,256,128]{2,1,0:T(8,128)} %broadcast_in_dim.15), calls=%async_computation.2 | async-start | bytes 2097152 | tf_op jit(solution)/shard_map/all_to_all | solution.py:15
  133.5 21.1 %all-to-all-start.4 = ((f32[16,256,1]{1,2,0:T(1,128)}), f32[16,256,1]{1,2,0:T(1,128)S(1)}, u32[]{:S(2)}, u32[]{:S(2)}) async-start(f32[16,256,1]{1,2,0:T(1,128)} %broadcast_in_dim.16), calls=%async_computation.4 | async-start | bytes 32768 | tf_op jit(solution)/shard_map/all_to_all | solution.py:15
  154.5 30.8 %all-to-all-start.3 = ((bf16[16,16,1376]{2,1,0:T(8,128)(2,1)}), bf16[16,16,1376]{2,1,0:T(8,128)(2,1)S(1)}, u32[]{:S(2)}, u32[]{:S(2)}) async-start(bf16[16,16,1376]{2,1,0:T(8,128)(2,1)} %bitcast.9), calls=%async_computation.3 | async-start | bytes 1441792 | tf_op jit(solution)/shard_map/all_to_all | solution.py:30
where the time goes:
time: 241 us
  waiting for transfers between devices  99.9 us (41%)
  blocking collectives  87.8 us (36%)
  starting transfers between devices  41.9 us (17%)
  local copies, waits for them, and re-layouts  5.44 us (2%)
  other arithmetic  3.91 us (2%)
    all_gather x2, blocking collectives, half_step(): hidden = lax.all_gather(own_hidden, 'ra', axis=0, tiled=True)  66.5 us
    all_to_all x2, waiting for transfers between devices, sum_at_owner(): lax.all_to_all(tiles, axis, split_axis=0, concat_axis=0, tiled=True)  62.1 us
    all_to_all x3, waiting for transfers between devices, sent_to_all(): return lax.all_to_all(copies, axis, split_axis=0, concat_axis=0, tiled=True)  37.8 us
    all_to_all x3, starting transfers between devices, sent_to_all(): return lax.all_to_all(copies, axis, split_axis=0, concat_axis=0, tiled=True)  34.6 us
    all_to_all x1, blocking collectives, sent_to_all(): return lax.all_to_all(copies, axis, split_axis=0, concat_axis=0, tiled=True)  21.3 us
    all_to_all x2, starting transfers between devices, sum_at_owner(): lax.all_to_all(tiles, axis, split_axis=0, concat_axis=0, tiled=True)  7.34 us
  transfers between devices with their start and end apart: 5, of which 5 were waited for; matrix products, arithmetic and copies ran while one was open for 2% of the time, Pallas kernels for 0%

commit v1 on v0

v1 whole, which is shorter than its diff:
```python
import functools

import jax
import jax.numpy as jnp
from jax import lax
from jax.experimental import pallas as pl
from jax.experimental.pallas import tpu as pltpu
from jax.sharding import PartitionSpec as P

MESH = pl.DeviceIdType.MESH
D = 2048
epsilon = 1e-06
residual_scale = 0.5

NZ, NY = 16, 8
ROWS = 32
TILE = 16
QUAD = (0, 1, 3, 2)
F32, BF16 = jnp.float32, jnp.bfloat16


def kernel(
    stream, gain, gate, up, down, gate_scale, up_scale, down_scale, out,
    xin, gain_v, gate_v, up_v, down_v, gs_v, us_v, ds_v,
    parts, w0, w1, xg, ob, rb, yb,
    in_sem, a_send, y_send, x_send, d_send, a_recv, y_recv, x_recv, d_recv,
    s_send, s_recv, o_send, o_recv, f_send, f_recv,
):
    z, y, d = lax.axis_index("ra"), lax.axis_index("cb"), lax.axis_index("dp")
    zq, zl = z // 4, z % 4
    x, c = d // 2, d % 2
    p = x % 2
    own = 2 * c + p
    classes = (own, 2 * c + 1 - p, 2 * (1 - c) + p, 2 * (1 - c) + 1 - p)
    weights = (w0, w1)

    def at_z(quad, low):
        return {"ra": 4 * ((zq + quad) % 4) + (zl + low) % 4}

    far_z = sorted(
        [(k, min(k, NZ - k)) for k in range(1, NZ)], key=lambda t: -t[1]
    )
    z_peers = [k for k, _ in far_z]
    y_plus, y_minus = {"cb": (y + 1) % NY}, {"cb": (y + NY - 1) % NY}
    x_plus, x_minus = {"dp": (d + 2) % 8}, {"dp": (d + 6) % 8}
    partner = {"dp": d + 1 - 2 * c}

    barrier = pltpu.get_barrier_semaphore()
    for k in z_peers:
        pl.semaphore_signal(barrier, 1, device_id={"ra": (z + k) % NZ}, device_id_type=MESH)
    for k in (4, 3, 5, 2, 6, 1, 7):
        pl.semaphore_signal(barrier, 1, device_id={"cb": (y + k) % NY}, device_id_type=MESH)
    for peer in (x_plus, x_minus, partner):
        pl.semaphore_signal(barrier, 1, device_id=peer, device_id_type=MESH)

    loads = [
        pltpu.make_async_copy(src, dst, in_sem.at[i])
        for i, (src, dst) in enumerate([
            (gate_scale, gs_v), (up_scale, us_v), (down_scale, ds_v), (gain, gain_v),
            (gate.at[0], gate_v.at[0]), (up.at[0], up_v.at[0]), (down.at[0], down_v.at[0]),
            (gate.at[1], gate_v.at[1]), (up.at[1], up_v.at[1]), (down.at[1], down_v.at[1]),
            (stream.at[pl.ds(pl.multiple_of(y * ROWS, ROWS), ROWS)], xin),
        ])
    ]
    for load in loads:
        load.start()
    for load in loads[:4]:
        load.wait()

    def put(b, m, j, tiles):
        count = tiles.shape[0] // TILE
        first, k = 8 * (j % 2), j // 2
        parts[b, first : first + count, m, TILE * k : TILE * (k + 1), :] = tiles.reshape(
            count, TILE, 128
        )

    def prepare(b):
        for m, (ref, scale) in enumerate(((gate_v, gs_v), (up_v, us_v))):
            loads[4 + 3 * b + m].wait()
            for j in range(6):
                width = 128 if j < 5 else 48
                cols = slice(128 * j, 128 * j + width)
                block = ref[b, :, cols] * scale[b : b + 1, cols]
                put(b, m, j, (block.T * gain_v[b : b + 1, :]).astype(BF16))
        loads[6 + 3 * b].wait()
        for j in range(6):
            height = 128 if j < 5 else 48
            block = down_v[b, 128 * j : 128 * j + height, :] * ds_v[b : b + 1, :]
            put(b, 2, j, block.astype(BF16))
        parts[b, 11:16, :, 2 * TILE :, :] = jnp.zeros((5, 3, TILE, 128), BF16)

    def copy(src, dst, send, recv, peer):
        return pltpu.make_async_remote_copy(
            src_ref=src, dst_ref=dst, send_sem=send, recv_sem=recv,
            device_id=peer, device_id_type=MESH,
        )

    def arrived(ref, sem):
        pltpu.make_async_copy(ref, ref, sem).wait()

    is_source = zl == own

    def spread_z(b):
        w = weights[b]

        @pl.when(is_source)
        def _():
            w[0, 0, 0] = parts[b, z]
            for quad in (2, 1, 3, 0):
                o = QUAD.index((4 - quad) % 4)
                for low in range(4):
                    if quad == 0 and low == 0:
                        continue
                    peer = at_z(quad, low)
                    copy(
                        parts.at[b, peer["ra"]], w.at[0, 0, o],
                        a_send.at[b], a_recv.at[b, o], peer,
                    ).start()

    def spread_tasks(b):
        w = weights[b]
        tasks = []

        def to_x(rel, o):
            copy(
                w.at[0, rel, o], w.at[1, rel, o], x_send.at[b], x_recv.at[b, rel, o],
                x_plus if o % 2 == 0 else x_minus,
            ).start()

        def to_y(rel, o, up_):
            there = (rel - 1) % NY if up_ else (rel + 1) % NY
            copy(
                w.at[0, rel, o], w.at[0, there, o], y_send.at[b], y_recv.at[b, there, o],
                y_plus if up_ else y_minus,
            ).start()

        def own_unit(o):
            if o == 0:
                @pl.when(jnp.logical_not(is_source))
                def _():
                    arrived(w.at[0, 0, 0], a_recv.at[b, 0])
            else:
                arrived(w.at[0, 0, o], a_recv.at[b, o])
            to_y(0, o, True)
            to_y(0, o, False)
            to_x(0, o)

        def ring_unit(s, o, up_):
            rel = (NY - s) if up_ else s
            arrived(w.at[0, rel, o], y_recv.at[b, rel, o])
            if s < 3 or (s == 3 and (o < 2) == up_):
                to_y(rel, o, up_)
            to_x(rel, o)

        def to_partner(cls, rel):
            copy(
                w.at[cls, rel], w.at[cls + 2, rel], d_send.at[b], d_recv.at[b, cls, rel], partner
            ).start()

        def own_done(rel):
            to_partner(0, rel)

        def x_done(rel):
            for o in range(4):
                arrived(w.at[1, rel, o], x_recv.at[b, rel, o])
            to_partner(1, rel)

        start = (0.0, 2.0, 2.5, 5.0)
        hop = 2.6
        for o in range(4):
            tasks.append((start[o], functools.partial(own_unit, o)))
            for s in range(1, 5):
                for up_ in (True, False):
                    if s < 4 or (o < 2) == up_:
                        tasks.append((start[o] + s * hop, functools.partial(ring_unit, s, o, up_)))
        for rel in range(NY):
            s = min(rel, NY - rel)
            tasks.append((start[3] + s * hop + 0.1, functools.partial(own_done, rel)))
            tasks.append((start[3] + (s + 1) * hop + 0.6, functools.partial(x_done, rel)))
        tasks.sort(key=lambda t: t[0])
        return [t for _, t in tasks]

    def spread_end(b):
        w = weights[b]
        for cls in range(2):
            for rel in range(NY):
                arrived(w.at[cls + 2, rel], d_recv.at[b, cls, rel])

    def source_of(cls, o):
        return 4 * ((zq + QUAD[o]) % 4) + classes[cls]

    def gather_start(b, own_rows):
        xg[b, z] = own_rows
        for k in z_peers:
            copy(
                xin if b == 0 else yb.at[0], xg.at[b, z], s_send.at[b], s_recv.at[b],
                {"ra": (z + k) % NZ},
            ).start()

    def gather_wait(b):
        arrived(xg.at[b, 0:15], s_recv.at[b])

    def hidden_of(b):
        w = weights[b]
        squares = jnp.zeros((ROWS, 128), F32)
        for i in range(NZ):
            piece = xg[b, i].astype(F32)
            squares = squares + piece * piece
        inverse = lax.rsqrt(jnp.sum(squares, axis=1, keepdims=True) / D + epsilon)
        sums = []
        for m in range(2):
            total = jnp.zeros((ROWS, 384), F32)
            for o in (0, 1, 2, 3):
                for cls in (0, 2):
                    lhs = jnp.concatenate(
                        [xg[b, source_of(cls, o)], xg[b, source_of(cls + 1, o)]], axis=1
                    )
                    rhs = jnp.concatenate(
                        [w[cls + i, :, o, m].reshape(384, 128) for i in range(2)], axis=1
                    )
                    total = total + lax.dot_general(
                        lhs, rhs, (((1,), (1,)), ((), ())), preferred_element_type=F32
                    )
            sums.append(total * inverse)
        return (sums[0] / (1.0 + jnp.exp(-sums[0])) * sums[1]).astype(BF16)

    def scatter_start(b, hidden):
        w = weights[b]
        for o in (3, 1, 2, 0):
            for cls in (0, 2):
                rhs = jnp.concatenate(
                    [w[cls + i, :, o, 2].reshape(384, 128) for i in range(2)], axis=1
                )
                piece = jnp.dot(hidden, rhs, preferred_element_type=F32).astype(BF16)
                for i in range(2):
                    ob[b, source_of(cls + i, o)] = piece[:, 128 * i : 128 * (i + 1)]
        for k in z_peers:
            there = (z + k) % NZ
            copy(ob.at[b, there], rb.at[b, z], o_send.at[b], o_recv.at[b], {"ra": there}).start()
        rb[b, z] = ob[b, z]

    def scatter_end(b, rows):
        arrived(rb.at[b, 0:15], o_recv.at[b])
        total = residual_scale * rows.astype(F32)
        for i in range(NZ):
            total = total + rb[b, i].astype(F32)
        return total.astype(BF16)

    prepare(0)
    loads[10].wait()
    pl.semaphore_wait(barrier, 25)
    spread_z(0)
    gather_start(0, xin[...])
    prepare(1)
    tasks = spread_tasks(0)
    for task in tasks[: len(tasks) // 2]:
        task()
    spread_z(1)
    for task in tasks[len(tasks) // 2 :]:
        task()
    spread_end(0)
    gather_wait(0)
    hidden = hidden_of(0)
    scatter_start(0, hidden)
    for task in spread_tasks(1):
        task()
    rows = scatter_end(0, xin[...])
    yb[0] = rows
    gather_start(1, rows)
    spread_end(1)
    gather_wait(1)
    hidden = hidden_of(1)
    scatter_start(1, hidden)
    rows = scatter_end(1, rows)
    yb[1] = rows
    final = pl.ds(pl.multiple_of(y * ROWS, ROWS), ROWS)
    out[final, :] = rows
    for k in (4, 3, 5, 2, 6, 1, 7):
        copy(
            yb.at[1], out.at[final], f_send, f_recv, {"cb": (y + k) % NY}
        ).start()
    arrived(out.at[0 : 7 * ROWS], f_recv)

    for b in range(2):
        w = weights[b]

        @pl.when(is_source)
        def _():
            arrived(parts.at[b, 0:15], a_send.at[b])

        arrived(w.at[0, 0:7], y_send.at[b])
        arrived(w.at[0], x_send.at[b])
        arrived(w.at[0:2], d_send.at[b])
        arrived(xg.at[b, 0:15], s_send.at[b])
        arrived(ob.at[b, 0:15], o_send.at[b])
    arrived(out.at[0 : 7 * ROWS], f_send)


def on_device(
    stream, norm_gain, gate_weight, up_weight, down_weight, gate_scale, up_scale, down_scale
):
    dma = pltpu.SemaphoreType.DMA
    return pl.pallas_call(
        kernel,
        out_shape=jax.ShapeDtypeStruct((256, 128), BF16),
        in_specs=[pl.BlockSpec(memory_space=pl.ANY)] * 8,
        out_specs=pl.BlockSpec(memory_space=pltpu.VMEM),
        scratch_shapes=[
            pltpu.VMEM((ROWS, 128), BF16),
            pltpu.VMEM((2, 128), F32),
            pltpu.VMEM((2, 128, 688), F32),
            pltpu.VMEM((2, 128, 688), F32),
            pltpu.VMEM((2, 688, 128), F32),
            pltpu.VMEM((2, 688), F32),
            pltpu.VMEM((2, 688), F32),
            pltpu.VMEM((2, 128), F32),
            pltpu.VMEM((2, NZ, 3, 48, 128), BF16),
            pltpu.VMEM((4, NY, 4, 3, 48, 128), BF16),
            pltpu.VMEM((4, NY, 4, 3, 48, 128), BF16),
            pltpu.VMEM((2, NZ, ROWS, 128), BF16),
            pltpu.VMEM((2, NZ, ROWS, 128), BF16),
            pltpu.VMEM((2, NZ, ROWS, 128), BF16),
            pltpu.VMEM((2, ROWS, 128), BF16),
            dma((11,)),
            dma((2,)),
            dma((2,)),
            dma((2,)),
            dma((2,)),
            dma((2, 4)),
            dma((2, NY, 4)),
            dma((2, NY, 4)),
            dma((2, 2, NY)),
            dma((2,)),
            dma((2,)),
            dma((2,)),
            dma((2,)),
            dma,
            dma,
        ],
        name="two_half_steps",
        compiler_params=pltpu.CompilerParams(
            collective_id=0, has_side_effects=True, vmem_limit_bytes=48 * 1024 * 1024
        ),
    )(stream, norm_gain, gate_weight, up_weight, down_weight, gate_scale, up_scale, down_scale)


def solution(mesh):
    in_specs = (
        P("dp", "ra"),
        P(None, "ra"),
        P(None, "ra", "cb"),
        P(None, "ra", "cb"),
        P(None, "cb", "ra"),
        P(None, "cb"),
        P(None, "cb"),
        P(None, "ra"),
    )
    out_specs = P("dp", "ra")
    return jax.shard_map(
        on_device, mesh=mesh, in_specs=in_specs, out_specs=out_specs, check_vma=False
    )
```

time: 241 us -> 107 us (0.44)
  the two profiles are of different devices: /device:TPU:4 before, /device:TPU:8 now
where the time goes in v1:
time: 107 us
  Pallas kernels  103 us (96%)
  local copies, waits for them, and re-layouts  3.13 us (3%)
    pallas_call x1, Pallas kernels, on_device(): pl.pallas_call(kernel, out_shape=jax.ShapeDtypeStruct((256, 128), BF16),...  103 us
    unnamed x17, local copies, waits for them, and re-layouts  3.13 us

profile of v1, /device:TPU:8, one launch (start us, length us, event | category | flops | bytes accessed | tf_op | source)
XLA Modules:
  0.0 106.7 jit_solution(10929022964127208335)
XLA Ops:
  0.0 0.0 copy-start.6
  0.0 1.4 %copy.9.gate = f32[2,128,688]{2,1,0:T(8,128)S(1)} copy(f32[2,128,688]{1,2,0:T(8,128)} %param.10) | data formatting | bytes 1409024 | tf_op args[2]
  1.4 0.0 copy-done.6
  1.5 0.0 copy-start
  1.5 0.0 copy-start.1
  1.5 0.0 copy-start.2
  1.5 0.0 copy-start.3
  1.5 0.0 copy-start.4
  1.5 0.0 copy-start.5
  1.5 0.3 copy.10.up
  1.8 0.8 copy-done
  2.6 0.0 copy-done.1
  2.6 0.0 copy-done.2
  2.6 0.0 copy-done.3
  2.6 0.0 copy-done.4
  2.6 0.0 copy-done.5
  2.6 103.4 %two_half_steps.1 = bf16[256,128]{1,0:T(8,128)(2,1)S(1)} custom-call(bf16[256,128]{1,0:T(8,128)(2,1)S(1)} %copy-done.1, f32[2,128]{1,0:T(2,128)S(1)} %copy-done.4, f32[2,128,688]{2,1,0:T(8,128)S(1)} %copy.9.gate, f32[2,128,688]{2,1,0:T(8,128)S(1)} %copy.10.up, f32[2,688,128]{2,1,0:T(8,128)S(1)} %copy-done, f32[2,688]{1,0:T(2,128)S(1)} %copy-done.2, ...), custom_call_target="tpu_custom_call" | custom-call | tf_op jit(solution)/shard_map/two_half_steps/pallas_call | solution.py:303
  106.0 0.6 copy.12
Async XLA Ops:
  0.0 1.4 %copy-start.6 = (f32[2,128,688]{1,2,0:T(8,128)S(1)}, f32[2,128,688]{1,2,0:T(8,128)}, u32[]{:S(2)}) copy-start(f32[2,128,688]{1,2,0:T(8,128)} %param.11) | copy-start | bytes 2113540
  1.5 1.1 %copy-start = (f32[2,688,128]{2,1,0:T(8,128)S(1)}, f32[2,688,128]{2,1,0:T(8,128)}, u32[]{:S(2)}) copy-start(f32[2,688,128]{2,1,0:T(8,128)} %down.1) | copy-start | bytes 2113540
  1.5 1.1 %copy-start.1 = (bf16[256,128]{1,0:T(8,128)(2,1)S(1)}, bf16[256,128]{1,0:T(8,128)(2,1)}, u32[]{:S(2)}) copy-start(bf16[256,128]{1,0:T(8,128)(2,1)} %stream.1) | copy-start | bytes 196612
  1.5 1.1 %copy-start.2 = (f32[2,688]{1,0:T(2,128)S(1)}, f32[2,688]{1,0:T(2,128)}, u32[]{:S(2)}) copy-start(f32[2,688]{1,0:T(2,128)} %gate_scale.1) | copy-start | bytes 16516
  1.5 1.1 %copy-start.3 = (f32[2,688]{1,0:T(2,128)S(1)}, f32[2,688]{1,0:T(2,128)}, u32[]{:S(2)}) copy-start(f32[2,688]{1,0:T(2,128)} %up_scale.1) | copy-start | bytes 16516
  1.5 1.1 %copy-start.4 = (f32[2,128]{1,0:T(2,128)S(1)}, f32[2,128]{1,0:T(2,128)}, u32[]{:S(2)}) copy-start(f32[2,128]{1,0:T(2,128)} %gain.1) | copy-start | bytes 3076
  1.5 1.1 copy-start.5

commit v2 on v1

--- a/solution.py
+++ b/solution.py
@@ -16,6 +16,11 @@
 ROWS = 32
 TILE = 16
 QUAD = (0, 1, 3, 2)
+RING, SKIP, FORK = {1: 0, 2: 1, 3: 2, 4: 3}, {1: 0, 2: 0, 3: 2, 4: 3}, {1: 0, 2: 0, 3: 2, 4: 2}
+TREE = ((FORK, FORK, FORK, FORK), (RING, RING, RING, RING))
+START = (0.0, 4.0, 4.5, 7.0)
+HOP = (2.7, 3.4)
+LAG = 10.0
 F32, BF16 = jnp.float32, jnp.bfloat16
 
 
@@ -77,11 +82,12 @@
     def prepare(b):
         for m, (ref, scale) in enumerate(((gate_v, gs_v), (up_v, us_v))):
             loads[4 + 3 * b + m].wait()
+            column = scale[...].T[:, b : b + 1]
             for j in range(6):
-                width = 128 if j < 5 else 48
-                cols = slice(128 * j, 128 * j + width)
-                block = ref[b, :, cols] * scale[b : b + 1, cols]
-                put(b, m, j, (block.T * gain_v[b : b + 1, :]).astype(BF16))
+                height = 128 if j < 5 else 48
+                span = slice(128 * j, 128 * j + height)
+                block = ref[b, span, :] * column[span] * gain_v[b : b + 1, :]
+                put(b, m, j, block.astype(BF16))
         loads[6 + 3 * b].wait()
         for j in range(6):
             height = 128 if j < 5 else 48
@@ -106,7 +112,7 @@
         @pl.when(is_source)
         def _():
             w[0, 0, 0] = parts[b, z]
-            for quad in (2, 1, 3, 0):
+            for quad in (0, 1, 3, 2):
                 o = QUAD.index((4 - quad) % 4)
                 for low in range(4):
                     if quad == 0 and low == 0:
@@ -127,12 +133,25 @@
                 x_plus if o % 2 == 0 else x_minus,
             ).start()
 
-        def to_y(rel, o, up_):
-            there = (rel - 1) % NY if up_ else (rel + 1) % NY
+        def to_y(rel, o, step):
+            there = (rel - step) % NY
             copy(
                 w.at[0, rel, o], w.at[0, there, o], y_send.at[b], y_recv.at[b, there, o],
-                y_plus if up_ else y_minus,
+                {"cb": (y + step) % NY},
             ).start()
+
+        def relay(o, offset):
+            for child in reach(o):
+                if parent_of(o, child) == offset:
+                    to_y(-offset % NY, o, child - offset)
+            to_x(-offset % NY, o)
+
+        def reach(o):
+            return (1, -1, 2, -2, 3, -3, 4 if o < 2 else -4)
+
+        def parent_of(o, offset):
+            size = TREE[b][o][abs(offset)]
+            return size if offset > 0 else -size
 
         def own_unit(o):
             if o == 0:
@@ -141,44 +160,39 @@
                     arrived(w.at[0, 0, 0], a_recv.at[b, 0])
             else:
                 arrived(w.at[0, 0, o], a_recv.at[b, o])
-            to_y(0, o, True)
-            to_y(0, o, False)
-            to_x(0, o)
-
-        def ring_unit(s, o, up_):
-            rel = (NY - s) if up_ else s
+            relay(o, 0)
+
+        def ring_unit(offset, o):
+            rel = -offset % NY
             arrived(w.at[0, rel, o], y_recv.at[b, rel, o])
-            if s < 3 or (s == 3 and (o < 2) == up_):
-                to_y(rel, o, up_)
-            to_x(rel, o)
+            relay(o, offset)
 
         def to_partner(cls, rel):
             copy(
                 w.at[cls, rel], w.at[cls + 2, rel], d_send.at[b], d_recv.at[b, cls, rel], partner
             ).start()
 
-        def own_done(rel):
-            to_partner(0, rel)
-
         def x_done(rel):
             for o in range(4):
                 arrived(w.at[1, rel, o], x_recv.at[b, rel, o])
             to_partner(1, rel)
 
-        start = (0.0, 2.0, 2.5, 5.0)
-        hop = 2.6
+        def time_of(o, offset):
+            if offset == 0:
+                return START[o]
+            parent = parent_of(o, offset)
+            return time_of(o, parent) + HOP[b] + 0.64 * abs(offset - parent)
+
         for o in range(4):
-            tasks.append((start[o], functools.partial(own_unit, o)))
-            for s in range(1, 5):
-                for up_ in (True, False):
-                    if s < 4 or (o < 2) == up_:
-                        tasks.append((start[o] + s * hop, functools.partial(ring_unit, s, o, up_)))
+            tasks.append((time_of(o, 0), functools.partial(own_unit, o)))
+            for offset in reach(o):
+                tasks.append((time_of(o, offset), functools.partial(ring_unit, offset, o)))
         for rel in range(NY):
-            s = min(rel, NY - rel)
-            tasks.append((start[3] + s * hop + 0.1, functools.partial(own_done, rel)))
-            tasks.append((start[3] + (s + 1) * hop + 0.6, functools.partial(x_done, rel)))
-        tasks.sort(key=lambda t: t[0])
-        return [t for _, t in tasks]
+            offset = rel if rel < 4 else NY - rel
+            last = max(time_of(o, offset) for o in range(4)) + 0.1
+            tasks.append((last, functools.partial(to_partner, 0, rel)))
+            tasks.append((last + HOP[b] + 1.0, functools.partial(x_done, rel)))
+        return tasks
 
     def spread_end(b):
         w = weights[b]
@@ -252,26 +266,29 @@
     spread_z(0)
     gather_start(0, xin[...])
     prepare(1)
-    tasks = spread_tasks(0)
-    for task in tasks[: len(tasks) // 2]:
-        task()
-    spread_z(1)
-    for task in tasks[len(tasks) // 2 :]:
-        task()
-    spread_end(0)
-    gather_wait(0)
-    hidden = hidden_of(0)
-    scatter_start(0, hidden)
-    for task in spread_tasks(1):
-        task()
-    rows = scatter_end(0, xin[...])
-    yb[0] = rows
-    gather_start(1, rows)
+    first, second = spread_tasks(0), [(t + LAG, f) for t, f in spread_tasks(1)]
+    second.append((LAG - 3.0, functools.partial(spread_z, 1)))
+    ready = max(t for t, _ in first)
+    rows = [None]
+
+    def block_0():
+        spread_end(0)
+        gather_wait(0)
+        scatter_start(0, hidden_of(0))
+
+    def between():
+        rows[0] = scatter_end(0, xin[...])
+        yb[0] = rows[0]
+        gather_start(1, rows[0])
+
+    steps = first + second + [(ready + 0.1, block_0), (ready + 10.0, between)]
+    for _, step in sorted(steps, key=lambda t: t[0]):
+        step()
     spread_end(1)
     gather_wait(1)
     hidden = hidden_of(1)
     scatter_start(1, hidden)
-    rows = scatter_end(1, rows)
+    rows = scatter_end(1, rows[0])
     yb[1] = rows
     final = pl.ds(pl.multiple_of(y * ROWS, ROWS), ROWS)
     out[final, :] = rows
@@ -308,8 +325,8 @@
         scratch_shapes=[
             pltpu.VMEM((ROWS, 128), BF16),
             pltpu.VMEM((2, 128), F32),
-            pltpu.VMEM((2, 128, 688), F32),
-            pltpu.VMEM((2, 128, 688), F32),
+            pltpu.VMEM((2, 688, 128), F32),
+            pltpu.VMEM((2, 688, 128), F32),
             pltpu.VMEM((2, 688, 128), F32),
             pltpu.VMEM((2, 688), F32),
             pltpu.VMEM((2, 688), F32),
@@ -339,9 +356,12 @@
         ],
         name="two_half_steps",
         compiler_params=pltpu.CompilerParams(
-            collective_id=0, has_side_effects=True, vmem_limit_bytes=48 * 1024 * 1024
+            collective_id=0, has_side_effects=True, vmem_limit_bytes=67043328
         ),
-    )(stream, norm_gain, gate_weight, up_weight, down_weight, gate_scale, up_scale, down_scale)
+    )(
+        stream, norm_gain, jnp.swapaxes(gate_weight, 1, 2), jnp.swapaxes(up_weight, 1, 2), down_weight,
+        gate_scale, up_scale, down_scale,
+    )
 
 
 def solution(mesh):

time: 107 us -> 94.3 us (0.88)
  Pallas kernels: 103 us -> 92.7 us
  local copies, waits for them, and re-layouts: 3.13 us -> 1.47 us
    pallas_call x1, Pallas kernels: 103 us -> 92.7 us  [on_device(): pl.pallas_call(kernel, out_shape=jax.ShapeDtypeStruct((256, 128), BF16),...]
    unnamed x17 -> x1, local copies, waits for them, and re-layouts: 3.13 us -> 1.47 us
where the time goes in v2:
time: 94.3 us; the launch traced here: 94.1 us
  Pallas kernels  92.7 us (98%)
  local copies, waits for them, and re-layouts  1.47 us (2%)
    pallas_call x1, Pallas kernels, on_device(): pl.pallas_call(kernel, out_shape=jax.ShapeDtypeStruct((256, 128), BF16),...  92.7 us

profile of v2, /device:TPU:8, one launch (start us, length us, event | category | flops | bytes accessed | tf_op | source)
XLA Modules:
  0.0 94.1 jit_solution(12563787046999958543)
XLA Ops:
  0.0 92.7 %two_half_steps.1 = bf16[256,128]{1,0:T(8,128)(2,1)} custom-call(bf16[256,128]{1,0:T(8,128)(2,1)} %stream.1, f32[2,128]{1,0:T(2,128)} %gain.1, f32[2,688,128]{2,1,0:T(8,128)} %bitcast.2, f32[2,688,128]{2,1,0:T(8,128)} %bitcast.3, f32[2,688,128]{2,1,0:T(8,128)} %down.1, f32[2,688]{1,0:T(2,128)} %gate_scale.1, f32[2,688]{1,0:T(2,128)} %up_scale.1, ...), custom_call_target="tpu_custom_call" | custom-call | tf_op jit(solution)/shard_map/two_half_steps/pallas_call | solution.py:320
  92.7 1.5 %copy.10 = bf16[256,128]{1,0:T(8,128)(2,1)} copy(bf16[256,128]{1,0:T(8,128)(2,1)} %two_half_steps.1) | data formatting | bytes 131072

commit v3 on v2

--- a/solution.py
+++ b/solution.py
@@ -17,10 +17,11 @@
 TILE = 16
 QUAD = (0, 1, 3, 2)
 RING, SKIP, FORK = {1: 0, 2: 1, 3: 2, 4: 3}, {1: 0, 2: 0, 3: 2, 4: 3}, {1: 0, 2: 0, 3: 2, 4: 2}
-TREE = ((FORK, FORK, FORK, FORK), (RING, RING, RING, RING))
-START = (0.0, 4.0, 4.5, 7.0)
-HOP = (2.7, 3.4)
-LAG = 10.0
+TREE = ((SKIP, SKIP, SKIP, FORK), (RING, RING, RING, RING))
+START = ((0.0, 4.0, 4.5, 7.0), (0.0, 0.3, 0.6, 0.9))
+HOP = (2.7, 3.6)
+AHEAD = 3.0
+NEAR, FAR = (4, 12, 3, 13, 2, 14, 1, 15), (8, 7, 9, 6, 10, 5, 11)
 F32, BF16 = jnp.float32, jnp.bfloat16
 
 
@@ -29,7 +30,7 @@
     xin, gain_v, gate_v, up_v, down_v, gs_v, us_v, ds_v,
     parts, w0, w1, xg, ob, rb, yb,
     in_sem, a_send, y_send, x_send, d_send, a_recv, y_recv, x_recv, d_recv,
-    s_send, s_recv, o_send, o_recv, f_send, f_recv,
+    s_send, s_recv, o_send, o_recv, f_send, f_recv, far_sem,
 ):
     z, y, d = lax.axis_index("ra"), lax.axis_index("cb"), lax.axis_index("dp")
     zq, zl = z // 4, z % 4
@@ -39,9 +40,6 @@
     classes = (own, 2 * c + 1 - p, 2 * (1 - c) + p, 2 * (1 - c) + 1 - p)
     weights = (w0, w1)
 
-    def at_z(quad, low):
-        return {"ra": 4 * ((zq + quad) % 4) + (zl + low) % 4}
-
     far_z = sorted(
         [(k, min(k, NZ - k)) for k in range(1, NZ)], key=lambda t: -t[1]
     )
@@ -51,7 +49,7 @@
     partner = {"dp": d + 1 - 2 * c}
 
     barrier = pltpu.get_barrier_semaphore()
-    for k in z_peers:
+    for k in NEAR:
         pl.semaphore_signal(barrier, 1, device_id={"ra": (z + k) % NZ}, device_id_type=MESH)
     for k in (4, 3, 5, 2, 6, 1, 7):
         pl.semaphore_signal(barrier, 1, device_id={"cb": (y + k) % NY}, device_id_type=MESH)
@@ -106,31 +104,30 @@
 
     is_source = zl == own
 
-    def spread_z(b):
+    def spread_z(b, steps):
         w = weights[b]
 
         @pl.when(is_source)
         def _():
-            w[0, 0, 0] = parts[b, z]
-            for quad in (0, 1, 3, 2):
-                o = QUAD.index((4 - quad) % 4)
-                for low in range(4):
-                    if quad == 0 and low == 0:
-                        continue
-                    peer = at_z(quad, low)
-                    copy(
-                        parts.at[b, peer["ra"]], w.at[0, 0, o],
-                        a_send.at[b], a_recv.at[b, o], peer,
-                    ).start()
+            if 1 in steps:
+                w[0, 0, 0] = parts[b, z]
+            for k in steps:
+                there = (z + k) % NZ
+                diff = (zq + 4 - there // 4) % 4
+                o = diff + diff // 2 - 2 * (diff // 3)
+                copy(
+                    parts.at[b, there], w.at[0, 0, o], a_send.at[b], a_recv.at[b, o], {"ra": there}
+                ).start()
 
     def spread_tasks(b):
         w = weights[b]
         tasks = []
 
         def to_x(rel, o):
+            side = (o + min(rel, NY - rel) + rel // 5) % 2
             copy(
                 w.at[0, rel, o], w.at[1, rel, o], x_send.at[b], x_recv.at[b, rel, o],
-                x_plus if o % 2 == 0 else x_minus,
+                x_plus if side == 0 else x_minus,
             ).start()
 
         def to_y(rel, o, step):
@@ -179,7 +176,7 @@
 
         def time_of(o, offset):
             if offset == 0:
-                return START[o]
+                return START[b][o]
             parent = parent_of(o, offset)
             return time_of(o, parent) + HOP[b] + 0.64 * abs(offset - parent)
 
@@ -214,44 +211,69 @@
     def gather_wait(b):
         arrived(xg.at[b, 0:15], s_recv.at[b])
 
-    def hidden_of(b):
-        w = weights[b]
+    def inverse_of(b):
         squares = jnp.zeros((ROWS, 128), F32)
         for i in range(NZ):
             piece = xg[b, i].astype(F32)
             squares = squares + piece * piece
-        inverse = lax.rsqrt(jnp.sum(squares, axis=1, keepdims=True) / D + epsilon)
+        return lax.rsqrt(jnp.sum(squares, axis=1, keepdims=True) / D + epsilon)
+
+    def sums_of(b, cls):
+        w = weights[b]
         sums = []
         for m in range(2):
             total = jnp.zeros((ROWS, 384), F32)
-            for o in (0, 1, 2, 3):
-                for cls in (0, 2):
-                    lhs = jnp.concatenate(
-                        [xg[b, source_of(cls, o)], xg[b, source_of(cls + 1, o)]], axis=1
-                    )
-                    rhs = jnp.concatenate(
-                        [w[cls + i, :, o, m].reshape(384, 128) for i in range(2)], axis=1
-                    )
-                    total = total + lax.dot_general(
-                        lhs, rhs, (((1,), (1,)), ((), ())), preferred_element_type=F32
-                    )
-            sums.append(total * inverse)
-        return (sums[0] / (1.0 + jnp.exp(-sums[0])) * sums[1]).astype(BF16)
+            for o in range(4):
+                lhs = jnp.concatenate(
+                    [xg[b, source_of(cls, o)], xg[b, source_of(cls + 1, o)]], axis=1
+                )
+                rhs = jnp.concatenate(
+                    [w[cls + i, :, o, m].reshape(384, 128) for i in range(2)], axis=1
+                )
+                total = total + lax.dot_general(
+                    lhs, rhs, (((1,), (1,)), ((), ())), preferred_element_type=F32
+                )
+            sums.append(total)
+        return sums
+
+    def activate(sums, more, inverse):
+        gate_sum, up_sum = ((a + c) * inverse for a, c in zip(sums, more))
+        return (gate_sum / (1.0 + jnp.exp(-gate_sum)) * up_sum).astype(BF16)
 
     def scatter_start(b, hidden):
         w = weights[b]
-        for o in (3, 1, 2, 0):
+        late = None
+
+        def send(quad, cls):
+            for i in range(2):
+                there = 4 * quad + classes[cls + i]
+
+                @pl.when(there != z)
+                def _():
+                    copy(
+                        ob.at[b, there], rb.at[b, z], o_send.at[b], o_recv.at[b], {"ra": there}
+                    ).start()
+
+        for step in range(4):
+            if b == 0:
+                o = (3, 1, 2, 0)[step]
+                quad = (zq + QUAD[o]) % 4
+            else:
+                quad = step
+                diff = (quad + 4 - zq) % 4
+                o = diff + diff // 2 - 2 * (diff // 3)
             for cls in (0, 2):
                 rhs = jnp.concatenate(
                     [w[cls + i, :, o, 2].reshape(384, 128) for i in range(2)], axis=1
                 )
                 piece = jnp.dot(hidden, rhs, preferred_element_type=F32).astype(BF16)
                 for i in range(2):
-                    ob[b, source_of(cls + i, o)] = piece[:, 128 * i : 128 * (i + 1)]
-        for k in z_peers:
-            there = (z + k) % NZ
-            copy(ob.at[b, there], rb.at[b, z], o_send.at[b], o_recv.at[b], {"ra": there}).start()
+                    ob[b, 4 * quad + classes[cls + i]] = piece[:, 128 * i : 128 * (i + 1)]
+                if late is not None:
+                    send(*late)
+                late = (quad, cls)
         rb[b, z] = ob[b, z]
+        send(*late)
 
     def scatter_end(b, rows):
         arrived(rb.at[b, 0:15], o_recv.at[b])
@@ -262,19 +284,26 @@
 
     prepare(0)
     loads[10].wait()
-    pl.semaphore_wait(barrier, 25)
-    spread_z(0)
+    pl.semaphore_wait(barrier, len(NEAR) + 10)
+    for k in (4, 12):
+        pl.semaphore_signal(far_sem, 1, device_id={"ra": (z + k) % NZ}, device_id_type=MESH)
+    spread_z(0, NEAR)
+    prepare(1)
+    pl.semaphore_wait(far_sem, 2)
+    spread_z(0, FAR)
     gather_start(0, xin[...])
-    prepare(1)
-    first, second = spread_tasks(0), [(t + LAG, f) for t, f in spread_tasks(1)]
-    second.append((LAG - 3.0, functools.partial(spread_z, 1)))
+    first = spread_tasks(0)
     ready = max(t for t, _ in first)
+    second = [(t + ready - AHEAD, f) for t, f in spread_tasks(1)]
+    second.append((5.0, functools.partial(spread_z, 1, NEAR[::-1] + FAR)))
     rows = [None]
 
     def block_0():
+        gather_wait(0)
+        inverse = inverse_of(0)
+        sums = sums_of(0, 0)
         spread_end(0)
-        gather_wait(0)
-        scatter_start(0, hidden_of(0))
+        scatter_start(0, activate(sums, sums_of(0, 2), inverse))
 
     def between():
         rows[0] = scatter_end(0, xin[...])
@@ -286,8 +315,8 @@
         step()
     spread_end(1)
     gather_wait(1)
-    hidden = hidden_of(1)
-    scatter_start(1, hidden)
+    inverse = inverse_of(1)
+    scatter_start(1, activate(sums_of(1, 0), sums_of(1, 2), inverse))
     rows = scatter_end(1, rows[0])
     yb[1] = rows
     final = pl.ds(pl.multiple_of(y * ROWS, ROWS), ROWS)
@@ -296,8 +325,6 @@
         copy(
             yb.at[1], out.at[final], f_send, f_recv, {"cb": (y + k) % NY}
         ).start()
-    arrived(out.at[0 : 7 * ROWS], f_recv)
-
     for b in range(2):
         w = weights[b]
 
@@ -310,6 +337,7 @@
         arrived(w.at[0:2], d_send.at[b])
         arrived(xg.at[b, 0:15], s_send.at[b])
         arrived(ob.at[b, 0:15], o_send.at[b])
+    arrived(out.at[0 : 7 * ROWS], f_recv)
     arrived(out.at[0 : 7 * ROWS], f_send)
 
 
@@ -353,6 +381,7 @@
             dma((2,)),
             dma,
             dma,
+            pltpu.SemaphoreType.REGULAR,
         ],
         name="two_half_steps",
         compiler_params=pltpu.CompilerParams(

time: 94.3 us -> 91.2 us (0.967)
  the two profiles are of different devices: /device:TPU:8 before, /device:TPU:1 now
where the time goes in v3:
time: 91.2 us; the launch traced here: 91 us
  Pallas kernels  89.5 us (98%)
  local copies, waits for them, and re-layouts  1.47 us (2%)
    pallas_call x1, Pallas kernels, on_device(): pl.pallas_call(kernel, out_shape=jax.ShapeDtypeStruct((256, 128), BF16),...  89.5 us

profile of v3, /device:TPU:1, one launch (start us, length us, event | category | flops | bytes accessed | tf_op | source)
XLA Modules:
  0.0 91.0 jit_solution(2260252271641284208)
XLA Ops:
  0.0 89.5 %two_half_steps.1 = bf16[256,128]{1,0:T(8,128)(2,1)} custom-call(bf16[256,128]{1,0:T(8,128)(2,1)} %stream.1, f32[2,128]{1,0:T(2,128)} %gain.1, f32[2,688,128]{2,1,0:T(8,128)} %bitcast.2, f32[2,688,128]{2,1,0:T(8,128)} %bitcast.3, f32[2,688,128]{2,1,0:T(8,128)} %down.1, f32[2,688]{1,0:T(2,128)} %gate_scale.1, f32[2,688]{1,0:T(2,128)} %up_scale.1, ...), custom_call_target="tpu_custom_call" | custom-call | tf_op jit(solution)/shard_map/two_half_steps/pallas_call | solution.py:348
  89.5 1.5 %copy.10 = bf16[256,128]{1,0:T(8,128)(2,1)} copy(bf16[256,128]{1,0:T(8,128)(2,1)} %two_half_steps.1) | data formatting | bytes 131072
